TPU v7x, 32 devices: a whole 2x2x4 slice. The times are simulated.
32 devices in a mesh: grp: 2 (over y), sp: 4 (over z), tp: 4 (over x, core).
Axes of the slice: x: 2, y: 2, z: 4, core: 2. Of those that a mesh axis runs over, the one named last changes fastest.
Arguments:
- queries: bfloat16 [6144, 1024], P(('grp', 'sp'), 'tp'), parts along dimension 0, may hold values from -8 to 8
- keys: bfloat16 [6144, 256], P(('grp', 'sp')), parts along dimension 0, may hold values from -8 to 8
- values: bfloat16 [6144, 256], P(('grp', 'sp')), parts along dimension 0, may hold values from -6 to 6
- query_gain: float32 [128], replicated, may hold values from 0.2 to 6
- key_gain: float32 [128], replicated, may hold values from 0.2 to 6
- residual: bfloat16 [6144, 2048], P(('grp', 'sp', 'tp')), parts along dimension 0, may hold values from -6 to 6
- out_weight: bfloat16 [1024, 2048], P('tp'), may hold values from -0.1875 to 0.1875
- mix_gain: float32 [2048], replicated, may hold values from 0.1 to 1.9
- ffn_gain: float32 [2048], replicated, may hold values from 0.1 to 1.9
- gate_in: bfloat16 [2048, 5632], P('sp', 'tp'), may hold values from -0.125 to 0.125
- value_in: bfloat16 [2048, 5632], P('sp', 'tp'), may hold values from -0.125 to 0.125
- conv_gate: float32 [3, 5632], P(None, 'tp'), may hold values from -3 to 3
- conv_value: float32 [3, 5632], P(None, 'tp'), may hold values from -3 to 3
- down_t: bfloat16 [2048, 5632], P('sp', 'tp'), may hold values from -0.078125 to 0.078125
Outputs:
- layer_out: bfloat16 [6144, 2048], P(('grp', 'sp', 'tp')), parts along dimension 0
There are 2 independent parts, one for each index of `grp`. A program takes and returns all parts, laid end to end along the dimension named above; an argument that names none is the same for every part. Nothing has to cross between parts.
All inputs are finite; a program needn't handle non-finite values.
Results may differ from a plain program's by a relative error of at most 0.02.
The roundings to bfloat16 on the way count: a program that leaves them out, or rounds other values in their place, can miss the bound.
Values may be sent and summed in bfloat16 or wider, within the bound.
A program may use at most 128 MiB of HBM per device.

v0:
```python
import jax
import jax.numpy as jnp
from jax import lax
from jax.sharding import PartitionSpec as P

HEADS = 8
KVH = 2
GRID_W = 64
EPSILON = 1e-06
THETA = 10000.0


def with_halo(block, sides, width):
    for axis, dim in sides:
        count = lax.axis_size(axis)
        forward = [(i, i + 1) for i in range(count - 1)]
        backward = [(target, source) for source, target in forward]
        low = lax.ppermute(
            lax.slice_in_dim(block, block.shape[dim] - width, None, axis=dim), axis, forward
        )
        high = lax.ppermute(lax.slice_in_dim(block, 0, width, axis=dim), axis, backward)
        block = jnp.concatenate([low, block, high], axis=dim)
    return block


def rotary_tables(positions, seq_total, head_dim):
    quarter = head_dim // 4
    inverse = THETA ** (-(2.0 * jnp.arange(quarter, dtype=jnp.float32)) / (head_dim // 2))
    grid_row = (positions // GRID_W - seq_total // GRID_W // 2).astype(jnp.float32)
    grid_col = (positions % GRID_W - GRID_W // 2).astype(jnp.float32)
    row_angle = grid_row[:, None] * inverse[None, :]
    col_angle = grid_col[:, None] * inverse[None, :]
    angle = jnp.concatenate([row_angle, row_angle, col_angle, col_angle], axis=-1)
    return (jnp.cos(angle), jnp.sin(angle))


def rotate_quarters(vector):
    first, second, third, fourth = jnp.split(vector, 4, axis=-1)
    return jnp.concatenate([-second, first, -fourth, third], axis=-1)


def prepare_heads(raw, gain, cos_table, sin_table, factor):
    floats = raw.astype(jnp.float32)
    normed = floats * lax.rsqrt(jnp.mean(floats * floats, axis=-1, keepdims=True) + EPSILON) * gain
    turned = normed * cos_table + rotate_quarters(normed) * sin_table
    return (turned * factor).astype(jnp.bfloat16)


def rms_rows(stream, gain):
    floats = stream.astype(jnp.float32)
    return floats * lax.rsqrt(jnp.mean(floats * floats, axis=-1, keepdims=True) + EPSILON) * gain


def body(
    queries,
    keys,
    values,
    query_gain,
    key_gain,
    residual,
    out_weight,
    mix_gain,
    ffn_gain,
    gate_in,
    value_in,
    conv_gate,
    conv_value,
    down_t,
):
    gate_rows, value_rows, down_rows = (
        lax.all_gather(gate_in, "sp", axis=0, tiled=True),
        lax.all_gather(value_in, "sp", axis=0, tiled=True),
        lax.all_gather(down_t, "sp", axis=0, tiled=True),
    )
    whole_out = lax.all_gather(out_weight, "tp", axis=0, tiled=True)
    tok_rows = queries.shape[0]
    head_dim = query_gain.shape[0]
    local_heads = queries.shape[1] // head_dim
    seq_total = tok_rows * lax.axis_size("sp")
    kv_head = lax.axis_index("tp") * local_heads // (HEADS // KVH)
    positions = lax.axis_index("sp") * tok_rows + jnp.arange(tok_rows, dtype=jnp.int32)
    cos_table, sin_table = rotary_tables(positions, seq_total, head_dim)
    key_own = lax.dynamic_slice_in_dim(keys, kv_head * head_dim, head_dim, 1)
    value_own = lax.dynamic_slice_in_dim(values, kv_head * head_dim, head_dim, 1)
    key_rot = prepare_heads(key_own, key_gain, cos_table, sin_table, 1.0)
    query_rot = prepare_heads(
        queries.reshape(tok_rows, local_heads, head_dim),
        query_gain,
        cos_table[:, None, :],
        sin_table[:, None, :],
        head_dim ** (-0.5),
    )
    query_rows = jnp.transpose(query_rot, (1, 0, 2)).reshape(local_heads * tok_rows, head_dim)
    query_count = local_heads * tok_rows
    running = jnp.full((query_count, 1), -1e30, jnp.float32)
    key_piece = lax.all_gather(key_rot, "sp", axis=0, tiled=True)
    value_piece = lax.all_gather(value_own, "sp", axis=0, tiled=True)
    scores = lax.dot_general(
        query_rows, key_piece, (((1,), (1,)), ((), ())), preferred_element_type=jnp.float32
    )
    newest = jnp.maximum(running, jnp.max(scores, axis=1, keepdims=True))
    weights = jnp.exp(scores - newest)
    denom = jnp.sum(weights, axis=1, keepdims=True)
    summed = jnp.dot(weights.astype(jnp.bfloat16), value_piece, preferred_element_type=jnp.float32)
    running, denom, summed = (newest, denom, summed)
    attended = (summed / denom).astype(jnp.bfloat16).reshape(local_heads, tok_rows, head_dim)
    attended = jnp.transpose(attended, (1, 0, 2)).reshape(tok_rows, local_heads * head_dim)
    own_rows = residual.shape[0]
    token_heads = lax.all_to_all(attended, "tp", split_axis=0, concat_axis=1, tiled=True)
    group_count = lax.axis_size("tp")
    group_cols = attended.shape[1]
    grouped_rows = token_heads.reshape(own_rows, group_count, group_cols)
    grouped_weight = whole_out.reshape(group_count, group_cols, whole_out.shape[1])
    partials = jnp.einsum(
        "rgc,gcd->grd", grouped_rows, grouped_weight, preferred_element_type=jnp.float32
    ).astype(jnp.bfloat16)
    mix = jnp.sum(partials.astype(jnp.float32), axis=0)
    stream = (residual.astype(jnp.float32) + rms_rows(mix, mix_gain)).astype(jnp.bfloat16)
    normed = rms_rows(stream, ffn_gain).astype(jnp.bfloat16)
    paired = jnp.concatenate([gate_rows, value_rows], axis=1)
    upward = jnp.dot(
        lax.all_gather(normed, "tp", axis=0, tiled=True), paired, preferred_element_type=jnp.float32
    ).astype(jnp.bfloat16)
    padded = with_halo(upward, (("sp", 0),), 1).astype(jnp.float32)
    taps = jnp.concatenate([conv_gate, conv_value], axis=1)
    mixed = taps[0] * padded[:-2] + taps[1] * padded[1:-1] + taps[2] * padded[2:]
    unit_cols = conv_gate.shape[1]
    hidden = (jax.nn.gelu(mixed[:, :unit_cols], approximate=True) * mixed[:, unit_cols:]).astype(
        jnp.bfloat16
    )
    ffn_out = lax.psum_scatter(
        lax.dot_general(
            hidden, down_rows, (((1,), (1,)), ((), ())), preferred_element_type=jnp.float32
        ).astype(jnp.bfloat16),
        "tp",
        scatter_dimension=0,
        tiled=True,
    ).astype(jnp.float32)
    return (stream.astype(jnp.float32) + ffn_out).astype(jnp.bfloat16)


def solution(mesh):
    return jax.shard_map(
        body,
        mesh=mesh,
        in_specs=(
            P(("grp", "sp"), "tp"),
            P(("grp", "sp"), None),
            P(("grp", "sp"), None),
            P(),
            P(),
            P(("grp", "sp", "tp"), None),
            P("tp", None),
            P(),
            P(),
            P("sp", "tp"),
            P("sp", "tp"),
            P(None, "tp"),
            P(None, "tp"),
            P("sp", "tp"),
        ),
        out_specs=P(("grp", "sp", "tp"), None),
        check_vma=False,
    )
```

profile of v0, /device:TPU:0, one launch (start us, length us, event | category | flops | bytes accessed | tf_op | source)
XLA Modules:
  0.0 454.8 jit_solution(9116688480287603135)
XLA Ops:
  8.8 1.1 fusion.43
  10.0 1.1 fusion.44
  11.8 2.0 fusion.46
  15.2 21.3 %all_gather.21 = bf16[3072,128]{1,0:T(8,128)(2,1)S(1)} all-gather(bf16[768,128]{1,0:T(8,128)(2,1)S(1)} %get-tuple-element.10), channel_id=1, replica_groups=mesh['grp'=2,'sp'=4,'tp'=4] {'sp'}, dimensions={0}, use_global_device_ids=true | all-gather | bytes 983040 | tf_op jit(solution)/shard_map/all_gather | solution.py:96
  36.5 8.0 %fusion.68 = (f32[1536]{0:T(1024)S(1)}, f32[1536,3072]{1,0:T(8,128)}) fusion(bf16[1536,128]{1,0:T(8,128)(2,1)S(1)} %bitcast.24, bf16[3072,128]{1,0:T(8,128)(2,1)S(1)} %all_gather.21), kind=kOutput, calls=%fused_computation.104 | convolution fusion | flops 1212676608 | bytes 20060160 | tf_op jit(solution)/shard_map/dot_general | solution.py:98
  44.5 18.4 %all_gather.22 = bf16[3072,128]{1,0:T(8,128)(2,1)S(1)} all-gather(bf16[768,128]{1,0:T(8,128)(2,1)S(1)} %constant_dynamic-slice_fusion), channel_id=1, replica_groups=mesh['grp'=2,'sp'=4,'tp'=4] {'sp'}, dimensions={0}, use_global_device_ids=true | all-gather | bytes 983040 | tf_op jit(solution)/shard_map/all_gather | solution.py:97
  62.8 9.0 %fusion = f32[1536]{0:T(1024)S(1)} fusion(f32[1536,3072]{1,0:T(8,128)} %get-tuple-element.26, f32[1536]{0:T(1024)S(1)} %broadcast_maximum_fusion), kind=kLoop, calls=%fused_computation.1 | loop fusion | flops 9435648 | bytes 18886656 | tf_op jit(solution)/shard_map/reduce_sum | solution.py:103
  71.9 9.2 %fusion.26 = bf16[1536,128]{1,0:T(8,128)(2,1)S(1)} fusion(bf16[3072,128]{1,0:T(8,128)(2,1)S(1)} %all_gather.22, f32[1536,3072]{1,0:T(8,128)} %get-tuple-element.26, f32[1536]{0:T(1024)S(1)} %broadcast_maximum_fusion, f32[1536]{0:T(1024)S(1)} %fusion), kind=kOutput, calls=%fused_computation.30 | convolution fusion | flops 1217789952 | bytes 20066304 | tf_op jit(solution)/shard_map/dot_general | solution.py:104
  81.8 9.9 %all_to_all.16 = bf16[4,192,256]{2,1,0:T(8,128)(2,1)S(1)} all-to-all(bf16[4,192,256]{2,1,0:T(8,128)(2,1)S(1)} %all_to_all.12), channel_id=1, replica_groups=mesh['grp'=2,'sp'=4,'tp'=4] {'tp'}, dimensions={0} | all-to-all | bytes 786432 | tf_op jit(solution)/shard_map/all_to_all | solution.py:109
  91.7 3.3 convert_reduce_fusion
  95.8 1.1 fusion.36
  97.6 57.5 %all-gather.10.cloned.1.call-done = bf16[2048,1408]{1,0:T(8,128)(2,1)} async-done(((bf16[512,1408]{1,0:T(8,128)(2,1)}), bf16[2048,1408]{1,0:T(8,128)(2,1)}) %all-gather.10.cloned.1.call-update) | async-done | bytes 5767184 | tf_op jit(solution)/shard_map/all_gather | solution.py:71
  155.1 106.9 %all-gather.12.cloned.1.call-done = bf16[2048,1408]{1,0:T(8,128)(2,1)} async-done(((bf16[512,1408]{1,0:T(8,128)(2,1)}), bf16[2048,1408]{1,0:T(8,128)(2,1)}) %all-gather.12.cloned.1.call-update) | async-done | bytes 5767184 | tf_op jit(solution)/shard_map/all_gather | solution.py:72
  262.0 28.2 %all-gather.8.cloned.1.call-done = bf16[768,2048]{1,0:T(8,128)(2,1)} async-done(((bf16[192,2048]{1,0:T(8,128)(2,1)}), bf16[768,2048]{1,0:T(8,128)(2,1)}) %all-gather.8.cloned.1.call-update) | async-done | bytes 3145744 | tf_op jit(solution)/shard_map/all_gather | solution.py:122
  290.2 13.8 %fusion.11 = bf16[768,2816]{1,0:T(8,128)(2,1)S(1)} fusion(bf16[768,2048]{1,0:T(8,128)(2,1)} %all-gather.8.cloned.1.call-done, bf16[2048,1408]{1,0:T(8,128)(2,1)} %all-gather.12.cloned.1.call-done, bf16[2048,1408]{1,0:T(8,128)(2,1)} %all-gather.10.cloned.1.call-done), kind=kOutput, calls=%fused_computation.16 | convolution fusion | flops 8883601408 | bytes 19005440 | tf_op jit(solution)/shard_map/dot_general | solution.py:121
  304.1 3.4 collective-permute-start
  307.5 1.3 collective-permute-start.1
  309.0 4.5 collective-permute-done.1
  313.5 1.2 maximum_convert_fusion
  314.7 4.7 %fusion.9 = f32[768,2816]{1,0:T(8,128)} fusion(f32[770,2816]{1,0:T(8,128)S(1)} %maximum_convert_fusion, f32[2816]{0:T(1024)S(1)} %get-tuple-element.6, f32[2816]{0:T(1024)S(1)} %get-tuple-element.7, f32[2816]{0:T(1024)S(1)} %get-tuple-element.5), kind=kLoop, calls=%fused_computation.10 | loop fusion | flops 10813440 | bytes 34636800 | tf_op jit(solution)/shard_map/add | solution.py:126
  319.4 79.2 %all-gather.14.cloned.1.call-done = bf16[2048,1408]{1,0:T(8,128)(2,1)} async-done(((bf16[512,1408]{1,0:T(8,128)(2,1)}), bf16[2048,1408]{1,0:T(8,128)(2,1)}) %all-gather.14.cloned.1.call-update) | async-done | bytes 5767184 | tf_op jit(solution)/shard_map/all_gather | solution.py:73
  398.6 10.8 %convolution_convert_fusion.1 = bf16[768,2048]{1,0:T(8,128)(2,1)} fusion(bf16[2048,1408]{1,0:T(8,128)(2,1)} %all-gather.14.cloned.1.call-done, f32[768,2816]{1,0:T(8,128)} %fusion.9), kind=kOutput, calls=%fused_computation.28 | convolution fusion | flops 4441571328 | bytes 17563648 | tf_op jit(solution)/shard_map/dot_general | solution.py:132
  409.4 36.2 %reduce-scatter.2.cloned.1.call-done = bf16[192,2048]{1,0:T(8,128)(2,1)} async-done(((bf16[768,2048]{1,0:T(8,128)(2,1)}), bf16[192,2048]{1,0:T(8,128)(2,1)}) %reduce-scatter.2.cloned.1.call-update) | async-done | bytes 786448 | tf_op jit(solution)/shard_map/reduce_scatter | solution.py:131
  445.6 2.3 fusion.37
  (62 shorter events, 6.5 us)
Async XLA Ops:
  6.5 8.6 %copy-start = (bf16[768,256]{1,0:T(8,128)(2,1)S(1)}, bf16[768,256]{1,0:T(8,128)(2,1)}, u32[]{:S(2)}) copy-start(bf16[768,256]{1,0:T(8,128)(2,1)} %param.16) | copy-start | bytes 1179652
  6.5 5.2 %copy-start.2 = (bf16[768,256]{1,0:T(8,128)(2,1)S(1)}, bf16[768,256]{1,0:T(8,128)(2,1)}, u32[]{:S(2)}) copy-start(bf16[768,256]{1,0:T(8,128)(2,1)} %param.15) | copy-start | bytes 1179652
  6.5 5.2 %copy-start.9 = (f32[128]{0:T(128)S(1)}, f32[128]{0:T(128)}, u32[]{:S(2)}) copy-start(f32[128]{0:T(128)} %param.18) | copy-start | bytes 1540
  6.5 85.2 %all-gather.6.cloned.1.call-start = ((), (), s32[]{:S(2)}) async-start(), calls=%async_computation.2 | async-start | bytes 5242880 | tf_op jit(solution)/shard_map/all_gather | solution.py:75
  7.3 147.8 %all-gather.10.cloned.1.call-start = ((), (), s32[]{:S(2)}) async-start(), calls=%async_computation.4 | async-start | bytes 7208960 | tf_op jit(solution)/shard_map/all_gather | solution.py:71
  8.0 254.0 %all-gather.12.cloned.1.call-start = ((), (), s32[]{:S(2)}) async-start(), calls=%async_computation.5 | async-start | bytes 7208960 | tf_op jit(solution)/shard_map/all_gather | solution.py:72
  8.7 281.5 %all-gather.8.cloned.1.call-start = ((), (), s32[]{:S(2)}) async-start(), calls=%async_computation.3 | async-start | bytes 3932160 | tf_op jit(solution)/shard_map/all_gather | solution.py:122
  11.1 3.0 copy-start.4
  11.4 3.0 copy-start.10
  91.7 3.6 copy-start.3
  91.7 3.6 copy-start.7
  95.0 0.7 copy-start.8
  95.1 2.5 copy-start.5
  95.1 2.5 copy-start.6
  97.0 301.6 %all-gather.14.cloned.1.call-start = ((), (), s32[]{:S(2)}) async-start(), calls=%async_computation.6 | async-start | bytes 7208960 | tf_op jit(solution)/shard_map/all_gather | solution.py:73
  97.5 348.1 %reduce-scatter.2.cloned.1.call-start = ((), (), s32[]{:S(2)}) async-start(), calls=%async_computation.7 | async-start | bytes 3932160 | tf_op jit(solution)/shard_map/reduce_scatter | solution.py:131
  304.1 4.9 %collective-permute-start = (bf16[1,2816]{1,0:T(2,128)(2,1)S(1)}, bf16[1,2816]{1,0:T(2,128)(2,1)S(1)}, u32[]{:S(2)}, u32[]{:S(2)}) collective-permute-start(bf16[1,2816]{1,0:T(2,128)(2,1)S(1)} %get-tuple-element.13), channel_id=1, source_target_pairs={{0,4},{4,8},{8,12},{1,5},{5,9},{9,13},{2,6},{6,10},{10,14},{3,7},{... | collective-permute-start | bytes 16904 | tf_op jit(solution)/shard_map/ppermute | solution.py:18
  307.5 6.0 %collective-permute-start.1 = (bf16[1,2816]{1,0:T(2,128)(2,1)S(1)}, bf16[1,2816]{1,0:T(2,128)(2,1)S(1)}, u32[]{:S(2)}, u32[]{:S(2)}) collective-permute-start(bf16[1,2816]{1,0:T(2,128)(2,1)S(1)} %get-tuple-element.14), channel_id=1, source_target_pairs={{4,0},{8,4},{12,8},{5,1},{9,5},{13,9},{6,2},{10,6},{14,10},{7,3},{... | collective-permute-start | bytes 16904 | tf_op jit(solution)/shard_map/ppermute | solution.py:21
  398.6 49.3 %copy-start.1 = (bf16[768,256]{1,0:T(8,128)(2,1)S(1)}, bf16[768,256]{1,0:T(8,128)(2,1)}, u32[]{:S(2)}) copy-start(bf16[768,256]{1,0:T(8,128)(2,1)} %param.16) | copy-start | bytes 1179652
Sparse Core Ops, SparseCore 0:
  8.9 37.1 all-gather.5
  47.7 107.3 all-gather.9
  156.7 105.2 all-gather.11
  263.4 26.7 all-gather.7
  291.6 106.9 all-gather.13
  409.5 36.0 reduce-scatter.1
where the time goes:
time: 455 us
  waiting for transfers between devices  315 us (69%)
  blocking collectives  49.6 us (11%)
  matrix products  45.2 us (10%)
  other arithmetic  24.4 us (5%)
  between operations  13.8 us (3%)
  starting transfers between devices  4.88 us (1%)
    all_gather x1, waiting for transfers between devices, body(): lax.all_gather(value_in, 'sp', axis=0, tiled=True)  107 us
    all_gather x1, waiting for transfers between devices, body(): lax.all_gather(down_t, 'sp', axis=0, tiled=True)  79.2 us
    all_gather x1, waiting for transfers between devices, body(): lax.all_gather(gate_in, 'sp', axis=0, tiled=True)  57.5 us
    reduce_scatter x1, waiting for transfers between devices, body(): lax.psum_scatter(lax.dot_general(hidden, down_rows, (((1,), (1,)), ((), (...  36.2 us
    all_gather x1, waiting for transfers between devices, body(): lax.all_gather(normed, 'tp', axis=0, tiled=True)  28.2 us
    all_gather x1, blocking collectives, body(): key_piece = lax.all_gather(key_rot, 'sp', axis=0, tiled=True)  21.3 us
    all_gather x1, blocking collectives, body(): value_piece = lax.all_gather(value_own, 'sp', axis=0, tiled=True)  18.4 us
    dot_general x1, matrix products, body(): jnp.dot(lax.all_gather(normed, 'tp', axis=0, tiled=True), paired, preferr...  13.8 us
  transfers between devices with their start and end apart: 8, of which 7 were waited for; matrix products, arithmetic and copies ran while one was open for 13% of the time, Pallas kernels for 0%

commit v1 on v0

--- a/solution.py
+++ b/solution.py
@@ -93,8 +93,11 @@
     query_rows = jnp.transpose(query_rot, (1, 0, 2)).reshape(local_heads * tok_rows, head_dim)
     query_count = local_heads * tok_rows
     running = jnp.full((query_count, 1), -1e30, jnp.float32)
-    key_piece = lax.all_gather(key_rot, "sp", axis=0, tiled=True)
-    value_piece = lax.all_gather(value_own, "sp", axis=0, tiled=True)
+    key_piece, value_piece = jnp.split(
+        lax.all_gather(jnp.concatenate([key_rot, value_own], axis=1), "sp", axis=0, tiled=True),
+        [key_rot.shape[1]],
+        axis=1,
+    )
     scores = lax.dot_general(
         query_rows, key_piece, (((1,), (1,)), ((), ())), preferred_element_type=jnp.float32
     )

time: 455 us -> 496 us (1.090)
  waiting for transfers between devices: 315 us -> 393 us
  blocking collectives: 49.6 us -> 9.89 us
    all_gather x1, waiting for transfers between devices: 57.5 us -> 99.1 us  [body(): lax.all_gather(gate_in, 'sp', axis=0, tiled=True)]
    all_gather x2 -> x0, blocking collectives: 39.7 us -> none  [the longest x1 21.3 us: body(): key_piece = lax.all_gather(key_rot, 'sp', axis=0, tiled=True)]
    all_gather x0 -> x1, waiting for transfers between devices: none -> 36.4 us  [body(): lax.all_gather(jnp.concatenate([key_rot, value_own], axis=1), 'sp', axis=...]
  transfers between devices with their start and end apart: 8 -> 9, of which waited for: 7 -> 8; matrix products, arithmetic and copies ran while one was open for 13% -> 11% of each run, Pallas kernels for 0% -> 0%
where the time goes in v1:
time: 496 us; the launch traced here: 495 us
  waiting for transfers between devices  393 us (79%)
  matrix products  47 us (9%)
  other arithmetic  25.6 us (5%)
  between operations  13.9 us (3%)
  blocking collectives  9.89 us (2%)
    all_gather x1, waiting for transfers between devices, body(): lax.all_gather(value_in, 'sp', axis=0, tiled=True)  106 us
    all_gather x1, waiting for transfers between devices, body(): lax.all_gather(gate_in, 'sp', axis=0, tiled=True)  99.1 us
    all_gather x1, waiting for transfers between devices, body(): lax.all_gather(down_t, 'sp', axis=0, tiled=True)  79.1 us
    all_gather x1, waiting for transfers between devices, body(): lax.all_gather(jnp.concatenate([key_rot, value_own], axis=1), 'sp', axis=...  36.4 us
    reduce_scatter x1, waiting for transfers between devices, body(): lax.psum_scatter(lax.dot_general(hidden, down_rows, (((1,), (1,)), ((), (...  36.2 us
    all_gather x1, waiting for transfers between devices, body(): lax.all_gather(normed, 'tp', axis=0, tiled=True)  28.2 us
    dot_general x1, matrix products, body(): jnp.dot(lax.all_gather(normed, 'tp', axis=0, tiled=True), paired, preferr...  13.8 us
    dot_general x1, matrix products, body(): lax.dot_general(hidden, down_rows, (((1,), (1,)), ((), ())), preferred_el...  10.7 us
  transfers between devices with their start and end apart: 9, of which 8 were waited for; matrix products, arithmetic and copies ran while one was open for 11% of the time, Pallas kernels for 0%

profile of v1, /device:TPU:0, one launch (start us, length us, event | category | flops | bytes accessed | tf_op | source)
XLA Modules:
  0.0 495.4 jit_solution(6911770089833920316)
XLA Ops:
  6.6 1.2 fusion.46
  7.8 1.1 fusion.47
  9.6 2.0 fusion.49
  11.6 0.8 pad_maximum_fusion.1
  15.9 36.4 %all-gather.7.cloned.1.call-done = bf16[3072,256]{1,0:T(8,128)(2,1)} async-done(((bf16[768,256]{1,0:T(8,128)(2,1)}), bf16[3072,256]{1,0:T(8,128)(2,1)}) %all-gather.7.cloned.1.call-update) | async-done | bytes 1572880 | tf_op jit(solution)/shard_map/all_gather | solution.py:97
  52.4 9.9 %fusion.71 = (f32[1536]{0:T(1024)S(1)}, f32[1536,3072]{1,0:T(8,128)}) fusion(bf16[1536,128]{1,0:T(8,128)(2,1)S(1)} %bitcast.22, bf16[3072,256]{1,0:T(8,128)(2,1)} %all-gather.7.cloned.1.call-done), kind=kOutput, calls=%fused_computation.108 | convolution fusion | flops 1212676608 | bytes 20060160 | tf_op jit(solution)/shard_map/dot_general | solution.py:101
  62.2 9.1 %fusion = f32[1536]{0:T(1024)S(1)} fusion(f32[1536,3072]{1,0:T(8,128)} %get-tuple-element.26, f32[1536]{0:T(1024)S(1)} %broadcast_maximum_fusion), kind=kLoop, calls=%fused_computation.1 | loop fusion | flops 9435648 | bytes 18886656 | tf_op jit(solution)/shard_map/reduce_sum | solution.py:106
  71.4 9.3 %fusion.26 = bf16[1536,128]{1,0:T(8,128)(2,1)S(1)} fusion(f32[1536,3072]{1,0:T(8,128)} %get-tuple-element.26, f32[1536]{0:T(1024)S(1)} %broadcast_maximum_fusion, bf16[3072,256]{1,0:T(8,128)(2,1)S(1)} %copy-done.2, f32[1536]{0:T(1024)S(1)} %fusion), kind=kOutput, calls=%fused_computation.30 | convolution fusion | flops 1217789952 | bytes 20070400 | tf_op jit(solution)/shard_map/dot_general | solution.py:107
  81.3 9.9 %all_to_all.16 = bf16[4,192,256]{2,1,0:T(8,128)(2,1)S(1)} all-to-all(bf16[4,192,256]{2,1,0:T(8,128)(2,1)S(1)} %all_to_all.12), channel_id=1, replica_groups=mesh['grp'=2,'sp'=4,'tp'=4] {'tp'}, dimensions={0} | all-to-all | bytes 786432 | tf_op jit(solution)/shard_map/all_to_all | solution.py:112
  91.2 3.3 convert_reduce_fusion
  95.3 1.1 fusion.36
  97.2 99.1 %all-gather.13.cloned.1.call-done = bf16[2048,1408]{1,0:T(8,128)(2,1)} async-done(((bf16[512,1408]{1,0:T(8,128)(2,1)}), bf16[2048,1408]{1,0:T(8,128)(2,1)}) %all-gather.13.cloned.1.call-update) | async-done | bytes 5767184 | tf_op jit(solution)/shard_map/all_gather | solution.py:71
  196.2 106.4 %all-gather.15.cloned.1.call-done = bf16[2048,1408]{1,0:T(8,128)(2,1)} async-done(((bf16[512,1408]{1,0:T(8,128)(2,1)}), bf16[2048,1408]{1,0:T(8,128)(2,1)}) %all-gather.15.cloned.1.call-update) | async-done | bytes 5767184 | tf_op jit(solution)/shard_map/all_gather | solution.py:72
  302.6 28.2 %all-gather.11.cloned.1.call-done = bf16[768,2048]{1,0:T(8,128)(2,1)} async-done(((bf16[192,2048]{1,0:T(8,128)(2,1)}), bf16[768,2048]{1,0:T(8,128)(2,1)}) %all-gather.11.cloned.1.call-update) | async-done | bytes 3145744 | tf_op jit(solution)/shard_map/all_gather | solution.py:125
  330.8 13.8 %fusion.11 = bf16[768,2816]{1,0:T(8,128)(2,1)S(1)} fusion(bf16[768,2048]{1,0:T(8,128)(2,1)} %all-gather.11.cloned.1.call-done, bf16[2048,1408]{1,0:T(8,128)(2,1)} %all-gather.15.cloned.1.call-done, bf16[2048,1408]{1,0:T(8,128)(2,1)} %all-gather.13.cloned.1.call-done), kind=kOutput, calls=%fused_computation.16 | convolution fusion | flops 8883601408 | bytes 19005440 | tf_op jit(solution)/shard_map/dot_general | solution.py:124
  344.7 3.4 collective-permute-start
  348.1 1.3 collective-permute-start.1
  349.7 4.5 collective-permute-done.1
  354.1 1.2 maximum_convert_fusion
  355.3 4.8 fusion.9
  360.1 79.1 %all-gather.17.cloned.1.call-done = bf16[2048,1408]{1,0:T(8,128)(2,1)} async-done(((bf16[512,1408]{1,0:T(8,128)(2,1)}), bf16[2048,1408]{1,0:T(8,128)(2,1)}) %all-gather.17.cloned.1.call-update) | async-done | bytes 5767184 | tf_op jit(solution)/shard_map/all_gather | solution.py:73
  439.2 10.7 %convolution_convert_fusion.1 = bf16[768,2048]{1,0:T(8,128)(2,1)} fusion(bf16[2048,1408]{1,0:T(8,128)(2,1)} %all-gather.17.cloned.1.call-done, f32[768,2816]{1,0:T(8,128)} %fusion.9), kind=kOutput, calls=%fused_computation.28 | convolution fusion | flops 4441571328 | bytes 17563648 | tf_op jit(solution)/shard_map/dot_general | solution.py:135
  450.0 36.2 %reduce-scatter.2.cloned.1.call-done = bf16[192,2048]{1,0:T(8,128)(2,1)} async-done(((bf16[768,2048]{1,0:T(8,128)(2,1)}), bf16[192,2048]{1,0:T(8,128)(2,1)}) %reduce-scatter.2.cloned.1.call-update) | async-done | bytes 786448 | tf_op jit(solution)/shard_map/reduce_scatter | solution.py:134
  486.2 2.3 fusion.37
  (66 shorter events, 6.4 us)
Async XLA Ops:
  6.5 2.8 copy-start
  6.5 3.1 copy-start.3
  6.5 3.1 copy-start.10
  6.5 45.8 %all-gather.7.cloned.1.call-start = ((), (), s32[]{:S(2)}) async-start(), calls=%async_computation.2 | async-start | bytes 1966080 | tf_op jit(solution)/shard_map/all_gather | solution.py:97
  9.6 5.3 %copy-start.5 = (bf16[768,256]{1,0:T(8,128)(2,1)S(1)}, bf16[768,256]{1,0:T(8,128)(2,1)}, u32[]{:S(2)}) copy-start(bf16[768,256]{1,0:T(8,128)(2,1)} %param.14) | copy-start | bytes 1179652
  11.6 3.6 copy-start.11
  12.5 78.8 %all-gather.9.cloned.1.call-start = ((), (), s32[]{:S(2)}) async-start(), calls=%async_computation.3 | async-start | bytes 5242880 | tf_op jit(solution)/shard_map/all_gather | solution.py:75
  13.2 183.0 %all-gather.13.cloned.1.call-start = ((), (), s32[]{:S(2)}) async-start(), calls=%async_computation.5 | async-start | bytes 7208960 | tf_op jit(solution)/shard_map/all_gather | solution.py:71
  14.0 288.7 %all-gather.15.cloned.1.call-start = ((), (), s32[]{:S(2)}) async-start(), calls=%async_computation.6 | async-start | bytes 7208960 | tf_op jit(solution)/shard_map/all_gather | solution.py:72
  14.5 316.3 %all-gather.11.cloned.1.call-start = ((), (), s32[]{:S(2)}) async-start(), calls=%async_computation.4 | async-start | bytes 3932160 | tf_op jit(solution)/shard_map/all_gather | solution.py:125
  62.2 9.2 %copy-start.2 = (bf16[3072,256]{1,0:T(8,128)(2,1)S(1)}, bf16[3072,256]{1,0:T(8,128)(2,1)}, u32[]{:S(2)}) copy-start(bf16[3072,256]{1,0:T(8,128)(2,1)} %all-gather.7.cloned.1.call-done) | copy-start | bytes 4718596
  91.2 3.6 copy-start.4
  91.2 3.6 copy-start.8
  94.6 0.7 copy-start.9
  94.6 2.5 copy-start.6
  94.6 2.5 copy-start.7
  96.5 342.7 %all-gather.17.cloned.1.call-start = ((), (), s32[]{:S(2)}) async-start(), calls=%async_computation.7 | async-start | bytes 7208960 | tf_op jit(solution)/shard_map/all_gather | solution.py:73
  97.1 389.2 %reduce-scatter.2.cloned.1.call-start = ((), (), s32[]{:S(2)}) async-start(), calls=%async_computation.8 | async-start | bytes 3932160 | tf_op jit(solution)/shard_map/reduce_scatter | solution.py:134
  344.7 4.9 collective-permute-start
  348.1 6.0 %collective-permute-start.1 = (bf16[1,2816]{1,0:T(2,128)(2,1)S(1)}, bf16[1,2816]{1,0:T(2,128)(2,1)S(1)}, u32[]{:S(2)}, u32[]{:S(2)}) collective-permute-start(bf16[1,2816]{1,0:T(2,128)(2,1)S(1)} %get-tuple-element.14), channel_id=1, source_target_pairs={{4,0},{8,4},{12,8},{5,1},{9,5},{13,9},{6,2},{10,6},{14,10},{7,3},{... | collective-permute-start | bytes 16904 | tf_op jit(solution)/shard_map/ppermute | solution.py:21
  439.2 49.3 %copy-start.1 = (bf16[768,256]{1,0:T(8,128)(2,1)S(1)}, bf16[768,256]{1,0:T(8,128)(2,1)}, u32[]{:S(2)}) copy-start(bf16[768,256]{1,0:T(8,128)(2,1)} %param.16) | copy-start | bytes 1179652
Sparse Core Ops, SparseCore 0:
  12.6 39.7 all-gather.6
  53.9 33.3 all-gather.8
  88.9 107.3 all-gather.12
  197.7 104.9 all-gather.14
  304.0 26.7 all-gather.10
  332.3 106.9 all-gather.16
  450.1 36.0 reduce-scatter.1
